TPU v7x, 32 devices: a whole 2x2x4 slice. The times are simulated.
32 devices in a mesh: ep: 16 (over z, y, x), tp: 2 (over core).
Axes of the slice: x: 2, y: 2, z: 4, core: 2. Of those that a mesh axis runs over, the one named last changes fastest.
Arguments:
- tokens: bfloat16 [112, 2304], P('ep'), may hold values from -6 to 6
- attn_gain: bfloat16 [2304], replicated, may hold values from 0.099609375 to 1.8984375
- query_weight: bfloat16 [2304, 2048], P(None, 'tp'), may hold values from -0.125 to 0.125
- key_weight: bfloat16 [2304, 2048], P(None, 'tp'), may hold values from -0.125 to 0.125
- value_weight: bfloat16 [2304, 2048], P(None, 'tp'), may hold values from -0.125 to 0.125
- out_weight: bfloat16 [2304, 2048], P(None, 'tp'), may hold values from -0.125 to 0.125
- lambdas: float32 [16], P('tp'), may hold values from 0.3 to 0.8
- head_gain: bfloat16 [128], replicated, may hold values from 0.099609375 to 1.8984375
- cache_keys: bfloat16 [112, 1024, 16, 128], P('ep', None, 'tp'), may hold values from -1500 to 1500
- cache_values: bfloat16 [112, 1024, 16, 128], P('ep', None, 'tp'), may hold values from -6 to 6
- lengths: int32 [112], P('ep'), may hold values from 2 to 1024, as said below
- moe_gain: bfloat16 [2304], replicated, may hold values from 0.099609375 to 1.8984375
- gate_weight: bfloat16 [16, 2304, 1024], P('ep', None, 'tp'), may hold values from -0.125 to 0.125
- up_weight: bfloat16 [16, 2304, 1024], P('ep', None, 'tp'), may hold values from -0.125 to 0.125
- down_weight: bfloat16 [16, 1024, 2304], P('ep', 'tp'), may hold values from -0.1875 to 0.1875
- shared_gate: bfloat16 [2304, 1024], P(None, 'tp'), may hold values from -0.125 to 0.125
- shared_up: bfloat16 [2304, 1024], P(None, 'tp'), may hold values from -0.125 to 0.125
- shared_down: bfloat16 [1024, 2304], P('tp'), may hold values from -0.1875 to 0.1875
- expert_ids: int32 [112, 6], P('ep'), may hold values from 0 to 15, all different within a row; in each aligned block of 7 rows (0 to 6, 7 to 13, ...) at most 5 rows name the same one
- expert_weights: float32 [112, 6], P('ep'), may hold values from 0.2 to 1
Outputs:
- result: bfloat16 [112, 2304], P('ep', 'tp')
Inputs may be any that keep to these rules, and one draw needn't show every extreme that they name: `expert_ids`: each row names 6 different experts. Among the rows of one device (aligned blocks of 7 rows) no expert is named by more than 5 rows, a bound that some block reaches. `lengths`: some sequence has 1024 cached positions.
All inputs are finite; a program needn't handle non-finite values.
Results may differ from a plain program's by a relative error of at most 0.02.
Values may be sent and summed in bfloat16 or wider, within the bound.
No kernel may reach another device: no remote copies, remote signals or barrier semaphores. Data moves between devices by JAX's collectives and lax.ppermute only.
A program may use at most 128 MiB of HBM per device.

v0:
```python
import jax
import jax.numpy as jnp
from jax import lax
from jax.sharding import PartitionSpec as P

epsilon = 1e-06


def rms_scale(values, gain):
    wide = values.astype(jnp.float32)
    return (
        wide
        * lax.rsqrt(jnp.mean(wide * wide, axis=-1, keepdims=True) + epsilon)
        * gain.astype(jnp.float32)
    )


def shards(
    tokens,
    attn_gain,
    query_weight,
    key_weight,
    value_weight,
    out_weight,
    lambdas,
    head_gain,
    cache_keys,
    cache_values,
    lengths,
    moe_gain,
    gate_weight,
    up_weight,
    down_weight,
    shared_gate,
    shared_up,
    shared_down,
    expert_ids,
    expert_weights,
):
    seq_dev, model_width = tokens.shape
    local_heads = lambdas.shape[0]
    head_dim = cache_keys.shape[-1] // 2
    cache_len = cache_keys.shape[1]
    normed = rms_scale(tokens, attn_gain).astype(jnp.bfloat16)
    query_rows = jnp.dot(normed, query_weight, preferred_element_type=jnp.float32).astype(
        jnp.bfloat16
    )
    key_new = jnp.dot(normed, key_weight, preferred_element_type=jnp.float32).astype(jnp.bfloat16)
    value_new = jnp.dot(normed, value_weight, preferred_element_type=jnp.float32).astype(
        jnp.bfloat16
    )
    score_scale = head_dim ** (-0.5)
    queries = query_rows.reshape(seq_dev, local_heads, 2, head_dim)
    new_keys = key_new.reshape(seq_dev, local_heads, 2, head_dim)
    new_values = value_new.reshape(seq_dev, local_heads, 2 * head_dim)
    past_keys = cache_keys.reshape(seq_dev, cache_len, local_heads, 2, head_dim)
    scores = (
        jnp.einsum("shmd,sjhmd->shmj", queries, past_keys, preferred_element_type=jnp.float32)
        * score_scale
    )
    own_score = (
        jnp.sum(queries.astype(jnp.float32) * new_keys.astype(jnp.float32), axis=-1) * score_scale
    )
    live_mask = (jnp.arange(cache_len, dtype=jnp.int32)[None, :] < lengths[:, None])[
        :, None, None, :
    ]
    peak_score = jnp.maximum(jnp.max(jnp.where(live_mask, scores, -jnp.inf), axis=-1), own_score)
    exp_terms = jnp.where(live_mask, jnp.exp(scores - peak_score[..., None]), 0.0)
    own_term = jnp.exp(own_score - peak_score)
    denom_sum = jnp.sum(exp_terms, axis=-1) + own_term
    map_probs = exp_terms / denom_sum[..., None]
    own_prob = own_term / denom_sum
    lambda_row = lambdas[None, :]
    mixture = (map_probs[:, :, 0] - lambda_row[..., None] * map_probs[:, :, 1]).astype(jnp.bfloat16)
    own_mixture = (own_prob[:, :, 0] - lambda_row * own_prob[:, :, 1]).astype(jnp.bfloat16)
    head_out = jnp.einsum(
        "shj,sjhv->shv", mixture, cache_values, preferred_element_type=jnp.float32
    )
    head_out = head_out + own_mixture.astype(jnp.float32)[..., None] * new_values.astype(
        jnp.float32
    )
    head_normed = (
        rms_scale(head_out, head_gain)
        .astype(jnp.bfloat16)
        .reshape(seq_dev, local_heads * 2 * head_dim)
    )
    attn_part = lax.dot_general(
        head_normed, out_weight, (((1,), (1,)), ((), ())), preferred_element_type=jnp.float32
    )
    attn_total = lax.psum(attn_part.astype(jnp.bfloat16), "tp").astype(jnp.float32)
    mixed_rows = (tokens.astype(jnp.float32) + attn_total).astype(jnp.bfloat16)
    moe_normed = rms_scale(mixed_rows, moe_gain).astype(jnp.bfloat16)
    shared_gate_out = jnp.dot(moe_normed, shared_gate, preferred_element_type=jnp.float32)
    shared_up_out = jnp.dot(moe_normed, shared_up, preferred_element_type=jnp.float32)
    shared_hidden = (jax.nn.silu(shared_gate_out) * shared_up_out).astype(jnp.bfloat16)
    shared_part = jnp.dot(shared_hidden, shared_down, preferred_element_type=jnp.float32)
    experts = lax.axis_size("ep")
    top_count = expert_ids.shape[1]
    capacity = min(seq_dev, max(2, 2 * seq_dev * top_count // experts))
    slot_count = seq_dev * top_count
    slot_ids = expert_ids.reshape(slot_count)
    expert_hits = (slot_ids[:, None] == jnp.arange(experts, dtype=jnp.int32)[None, :]).astype(
        jnp.int32
    )
    slot_rank = jnp.sum((jnp.cumsum(expert_hits, axis=0) - expert_hits) * expert_hits, axis=1)
    slot_place = slot_ids * capacity + slot_rank
    placed = (
        slot_place[:, None] == jnp.arange(experts * capacity, dtype=jnp.int32)[None, :]
    ).astype(jnp.bfloat16)
    slot_token = jnp.arange(slot_count, dtype=jnp.int32) // top_count
    token_pick = (slot_token[:, None] == jnp.arange(seq_dev, dtype=jnp.int32)[None, :]).astype(
        jnp.bfloat16
    )
    dispatch = lax.dot_general(
        placed, token_pick, (((0,), (0,)), ((), ())), preferred_element_type=jnp.float32
    ).astype(jnp.bfloat16)
    col_count = model_width // lax.axis_size("tp")
    own_start = lax.axis_index("tp") * col_count
    own_normed = lax.dynamic_slice_in_dim(moe_normed, own_start, col_count, 1)
    send_slice = jnp.dot(dispatch, own_normed, preferred_element_type=jnp.float32).astype(
        jnp.bfloat16
    )
    arrived = lax.all_to_all(send_slice, "ep", split_axis=0, concat_axis=0, tiled=True)
    received = lax.all_gather(arrived, "tp", axis=1, tiled=True)
    gate_out = jnp.dot(received, gate_weight[0], preferred_element_type=jnp.float32)
    up_out = jnp.dot(received, up_weight[0], preferred_element_type=jnp.float32)
    expert_hidden = (jax.nn.silu(gate_out) * up_out).astype(jnp.bfloat16)
    expert_part = jnp.dot(expert_hidden, down_weight[0], preferred_element_type=jnp.float32)
    expert_sum, shared_out = (
        lax.psum_scatter(
            expert_part.astype(jnp.bfloat16), "tp", scatter_dimension=1, tiled=True
        ).astype(jnp.float32),
        lax.psum_scatter(
            shared_part.astype(jnp.bfloat16), "tp", scatter_dimension=1, tiled=True
        ).astype(jnp.float32),
    )
    returned = lax.all_to_all(
        expert_sum.astype(jnp.bfloat16), "ep", split_axis=0, concat_axis=0, tiled=True
    )
    slot_values = jnp.dot(placed, returned, preferred_element_type=jnp.float32).reshape(
        seq_dev, top_count, col_count
    )
    routed = jnp.sum(expert_weights[:, :, None] * slot_values, axis=1)
    own_cols = lax.dynamic_slice_in_dim(mixed_rows, own_start, col_count, 1)
    return (own_cols.astype(jnp.float32) + routed + shared_out).astype(jnp.bfloat16)


def solution(mesh):
    in_specs = (
        P("ep", None),
        P(),
        P(None, "tp"),
        P(None, "tp"),
        P(None, "tp"),
        P(None, "tp"),
        P("tp"),
        P(),
        P("ep", None, "tp", None),
        P("ep", None, "tp", None),
        P("ep"),
        P(),
        P("ep", None, "tp"),
        P("ep", None, "tp"),
        P("ep", "tp", None),
        P(None, "tp"),
        P(None, "tp"),
        P("tp", None),
        P("ep", None),
        P("ep", None),
    )
    out_specs = P("ep", "tp")
    return jax.shard_map(shards, mesh=mesh, in_specs=in_specs, out_specs=out_specs, check_vma=False)
```

profile of v0, /device:TPU:0, one launch (start us, length us, event | category | flops | bytes accessed | tf_op | source)
XLA Modules:
  0.0 123.7 jit_solution(13733338271488698938)
XLA Ops:
  6.5 0.0 copy-start
  6.5 0.0 reduce-scatter.7.cloned.1.call-start
  6.5 0.8 convert_element_type.102
  7.4 0.9 fusion.36
  8.3 3.1 %convolution_convert_fusion.6 = bf16[7,1024]{1,0:T(8,128)(2,1)S(1)} fusion(bf16[2304,1024]{1,0:T(8,128)(2,1)} %param.22, bf16[7,2304]{1,0:T(8,128)(2,1)} %param.20, f32[2304]{0:T(1024)S(1)} %convert_element_type.102, f32[7]{0:T(128)S(1)} %add_rsqrt_fusion.2), kind=kOutput, calls=%fused_computation.20 | convolution fusion | flops 33101824 | bytes 4774428 | tf_op jit(solution)/shard_map/dot_general | solution.py:45
  11.4 0.1 reshape.146
  11.5 0.1 reshape.134
  11.6 0.0 copy-start.1
  11.6 20.6 %copy.40 = bf16[7,1024,8,128]{1,3,2,0:T(8,128)(2,1)} copy(bf16[7,1024,8,128]{3,2,1,0:T(8,128)(2,1)} %param.28) | data formatting | bytes 29360128 | tf_op args[8]
  32.2 0.1 iota_compare_fusion
  32.3 3.1 %fusion.18 = f32[7,1024]{1,0:T(8,128)S(1)} fusion(bf16[2304,1024]{1,0:T(8,128)(2,1)} %param.23, bf16[7,2304]{1,0:T(8,128)(2,1)S(1)} %copy-done.1, f32[2304]{0:T(1024)S(1)} %convert_element_type.102, f32[7]{0:T(128)S(1)} %add_rsqrt_fusion.2), kind=kOutput, calls=%fused_computation.19 | convolution fusion | flops 33108992 | bytes 4788764 | tf_op jit(solution)/shard_map/dot_general | solution.py:48
  35.4 0.1 reshape.137
  35.5 0.1 multiply_reduce_fusion
  35.7 0.1 copy.41
  35.8 7.3 %fusion.69 = f32[7,8,2,1,1024]{4,3,2,1,0:T(1,128)S(1)} fusion(bf16[7,8,2,64,1]{3,4,2,1,0:T(2,128)(2,1)S(1)} %reshape.146, bf16[7,1024,8,2,64]{1,4,3,2,0:T(8,128)(2,1)} %bitcast.87), kind=kOutput, calls=%fused_computation.101 | convolution fusion | flops 14680064 | bytes 15153152 | tf_op jit(solution)/shard_map/shmd,sjhmd->shmj/dot_general | solution.py:58
  43.1 0.3 select_reduce_fusion
  43.4 0.3 fusion.21
  43.7 0.2 fusion.20
  44.0 0.1 fusion.31
  44.2 0.0 slice-start.2
  44.2 0.8 fusion.17
  44.9 7.6 %fusion = f32[7,8,1,128]{3,2,1,0:T(1,128)S(1)} fusion(bf16[7,1024,8,128]{3,2,1,0:T(8,128)(2,1)} %param.29, bf16[7,8,1024,1]{2,1,0,3:T(8,128)(2,1)S(1)} %fusion.31), kind=kOutput, calls=%fused_computation | convolution fusion | flops 14680064 | bytes 14823424 | tf_op jit(solution)/shard_map/shj,sjhv->shv/dot_general | solution.py:76
  52.6 0.0 copy-start.3
  52.6 0.0 copy-start.2
  52.6 0.2 multiply_reduce_fusion.1
  52.7 0.0 copy-done.7
  52.8 0.1 fusion.52
  52.9 1.3 %convolution_convert_fusion.2 = bf16[7,2304]{1,0:T(8,128)(2,1)S(1)} fusion(bf16[2304,1024]{1,0:T(8,128)(2,1)S(1)} %bitcast.91, bf16[1,7,8,128]{3,2,1,0:T(8,128)(2,1)S(1)} %fusion.52), kind=kOutput, calls=%fused_computation.4 | convolution fusion | flops 33046272 | bytes 4765184 | tf_op jit(solution)/shard_map/dot_general | solution.py:87
  54.2 3.8 %psum.7 = bf16[7,2304]{1,0:T(8,128)(2,1)S(1)} all-reduce(bf16[7,2304]{1,0:T(8,128)(2,1)S(1)} %convolution_convert_fusion.2), channel_id=1, replica_groups=mesh['ep'=16,'tp'=2] {'tp'}, use_global_device_ids=true, to_apply=%region_5.6 | all-reduce | flops 16128 | bytes 64512 | tf_op jit(solution)/shard_map/psum | solution.py:90
  58.0 0.1 fusion.33
  58.1 0.1 eq.63
  58.2 0.1 fusion.41
  58.3 0.1 reduce_window_sum.11
  58.4 0.2 select_reduce_fusion.1
  58.6 0.1 fusion.35
  58.7 0.5 convolution_convert_fusion.3
  59.2 0.1 all_to_all.16
  59.2 19.0 %all_to_all.24 = bf16[16,5,1152]{2,1,0:T(8,128)(2,1)S(1)} all-to-all(bf16[16,5,1152]{2,1,0:T(8,128)(2,1)S(1)} %all_to_all.16), channel_id=1, replica_groups=mesh['ep'=16,'tp'=2] {'ep'}, dimensions={0} | all-to-all | bytes 368640 | tf_op jit(solution)/shard_map/all_to_all | solution.py:123
  78.3 0.1 all_to_all.18
  78.4 2.1 %all_gather.3 = bf16[80,2304]{1,0:T(8,128)(2,1)S(1)} all-gather(bf16[80,1152]{1,0:T(8,128)(2,1)S(1)} %all_to_all.18), channel_id=1, replica_groups=mesh['ep'=16,'tp'=2] {'tp'}, dimensions={1}, use_global_device_ids=true | all-gather | bytes 552960 | tf_op jit(solution)/shard_map/all_gather | solution.py:124
  80.4 2.2 %fusion.5 = f32[80,512]{1,0:T(8,128)S(1)} fusion(bf16[80,2304]{1,0:T(8,128)(2,1)S(1)} %all_gather.3, bf16[1,2304,512]{2,1,0:T(8,128)(2,1)} %param.32), kind=kOutput, calls=%fused_computation.8 | convolution fusion | flops 188743680 | bytes 2891776 | tf_op jit(solution)/shard_map/dot_general | solution.py:125
  82.6 2.6 %convolution_convert_fusion = bf16[80,2304]{1,0:T(8,128)(2,1)S(1)} fusion(bf16[1,512,2304]{2,1,0:T(8,128)(2,1)S(1)} %copy-done, bf16[80,2304]{1,0:T(8,128)(2,1)S(1)} %all_gather.3, bf16[1,2304,512]{2,1,0:T(8,128)(2,1)} %param.33, f32[80,512]{1,0:T(8,128)S(1)} %fusion.5), kind=kOutput, calls=%fused_computation.2 | convolution fusion | flops 377917440 | bytes 5619712 | tf_op jit(solution)/shard_map/dot_general | solution.py:128
  85.2 1.1 copy.50
  86.3 0.0 reduce-scatter.7.cloned.1.call-update
  86.3 0.0 copy-start.4
  86.3 2.1 %fusion.70 = f32[7,512]{1,0:T(8,128)S(1)} fusion(bf16[7,2304]{1,0:T(8,128)(2,1)S(1)} %fusion.35, bf16[2304,512]{1,0:T(8,128)(2,1)} %param.35), kind=kOutput, calls=%fused_computation.102 | convolution fusion | flops 16515072 | bytes 2405888 | tf_op jit(solution)/shard_map/dot_general | solution.py:93
  88.4 3.9 %reduce-scatter.7.cloned.1.call-done = bf16[1152,80]{1,0:T(8,128)(2,1)} async-done(((bf16[2304,80]{1,0:T(8,128)(2,1)}), bf16[1152,80]{1,0:T(8,128)(2,1)}) %reduce-scatter.7.cloned.1.call-update) | async-done | bytes 184336
  92.3 1.1 copy.51
  93.4 0.8 all_to_all.19
  94.2 6.7 %all-to-all-start.1 = ((bf16[16,5,1152]{2,1,0:T(8,128)(2,1)}), bf16[16,5,1152]{2,1,0:T(8,128)(2,1)S(1)}, u32[]{:S(2)}, u32[]{:S(2)}) async-start(bf16[16,5,1152]{2,1,0:T(8,128)(2,1)} %all_to_all.19), calls=%async_computation.1 | async-start | bytes 589824 | tf_op jit(solution)/shard_map/all_to_all | solution.py:137
  100.9 0.0 reduce-scatter.9.cloned.1.call-start
  101.0 3.2 %convolution_convert_fusion.1 = bf16[7,2304]{1,0:T(8,128)(2,1)S(1)} fusion(bf16[512,2304]{1,0:T(8,128)(2,1)} %param.37, bf16[7,2304]{1,0:T(8,128)(2,1)S(1)} %fusion.35, bf16[2304,512]{1,0:T(8,128)(2,1)} %param.36, f32[7,512]{1,0:T(8,128)S(1)} %fusion.70), kind=kOutput, calls=%fused_computation.3 | convolution fusion | flops 33067776 | bytes 4797440 | tf_op jit(solution)/shard_map/dot_general | solution.py:96
  104.2 1.1 copy.52
  105.3 0.0 reduce-scatter.9.cloned.1.call-update
  105.3 0.1 reduce_sum.70
  105.4 0.1 copy.44
  105.5 0.0 copy-done.4
  105.5 0.1 copy.43
  105.6 9.2 %reduce-scatter.9.cloned.1.call-done = bf16[1152,7]{1,0:T(8,128)(2,1)} async-done(((bf16[2304,7]{1,0:T(8,128)(2,1)}), bf16[1152,7]{1,0:T(8,128)(2,1)}) %reduce-scatter.9.cloned.1.call-update) | async-done | bytes 16144
  114.8 1.1 copy.53
  115.9 0.0 all-to-all-done.1
  115.9 0.1 reshape.144
  116.0 0.2 fusion.10
  116.2 0.6 add_convert_fusion
  (29 shorter events, 0.1 us)
Async XLA Ops:
  6.5 76.1 %copy-start = (bf16[1,512,2304]{2,1,0:T(8,128)(2,1)S(1)}, bf16[1,512,2304]{2,1,0:T(8,128)(2,1)}, u32[]{:S(2)}) copy-start(bf16[1,512,2304]{2,1,0:T(8,128)(2,1)} %param.34) | copy-start | bytes 7077892
  6.5 85.7 %reduce-scatter.7.cloned.1.call-start = ((), (), s32[]{:S(2)}) async-start(), calls=%async_computation.4 | async-start | bytes 884736
  11.6 20.6 %copy-start.6 = (s32[7]{0:T(128)S(1)}, s32[7]{0:T(128)}, u32[]{:S(2)}) copy-start(s32[7]{0:T(128)} %param.30) | copy-start | bytes 88
  11.6 20.7 %copy-start.1 = (bf16[7,2304]{1,0:T(8,128)(2,1)S(1)}, bf16[7,2304]{1,0:T(8,128)(2,1)}, u32[]{:S(2)}) copy-start(bf16[7,2304]{1,0:T(8,128)(2,1)} %param.20) | copy-start | bytes 96772
  32.3 11.9 %slice-start = ((s8[4718592]{0:T(1024)(128)(4,1)}), s8[524288]{0:T(1024)(128)(4,1)S(1)}, s32[]{:S(2)}) async-start(s8[4718592]{0:T(1024)(128)(4,1)} %bitcast.88), calls=%async_computation.6 | async-start | bytes 1048576
  35.8 8.2 %copy-start.5 = (f32[8]{0:T(128)S(1)}, f32[8]{0:T(128)}, u32[]{:S(2)}) copy-start(f32[8]{0:T(128)} %param.26) | copy-start | bytes 100
  35.8 8.3 %slice-start.1 = ((s8[4718592]{0:T(1024)(128)(4,1)}), s8[4194304]{0:T(1024)(128)(4,1)S(1)}, s32[]{:S(2)}) async-start(s8[4718592]{0:T(1024)(128)(4,1)} %bitcast.88), calls=%async_computation.7 | async-start | bytes 8388608
  44.2 8.7 %slice-start.2 = ((s8[4718592]{0:T(1024)(128)(4,1)}), s8[4194304]{0:T(1024)(128)(4,1)S(1)}, s32[]{:S(2)}) async-start(s8[4718592]{0:T(1024)(128)(4,1)} %bitcast.90), calls=%async_computation.8 | async-start | bytes 8388608
  44.9 7.8 %copy-start.7 = (bf16[128]{0:T(256)(128)(2,1)S(1)}, bf16[128]{0:T(256)(128)(2,1)}, u32[]{:S(2)}) copy-start(bf16[128]{0:T(256)(128)(2,1)} %param.27) | copy-start | bytes 772
  44.9 7.9 %slice-start.3 = ((s8[4718592]{0:T(1024)(128)(4,1)}), s8[524288]{0:T(1024)(128)(4,1)S(1)}, s32[]{:S(2)}) async-start(s8[4718592]{0:T(1024)(128)(4,1)} %bitcast.90), calls=%async_computation.9 | async-start | bytes 1048576
  52.6 5.6 %copy-start.3 = (bf16[2304]{0:T(1024)(128)(2,1)S(1)}, bf16[2304]{0:T(1024)(128)(2,1)}, u32[]{:S(2)}) copy-start(bf16[2304]{0:T(1024)(128)(2,1)} %param.31) | copy-start | bytes 13828
  52.6 5.6 %copy-start.2 = (s32[7,6]{1,0:T(8,128)S(1)}, s32[7,6]{1,0:T(8,128)}, u32[]{:S(2)}) copy-start(s32[7,6]{1,0:T(8,128)} %param.38) | copy-start | bytes 508
  86.3 19.2 %copy-start.4 = (f32[7,6]{1,0:T(8,128)S(1)}, f32[7,6]{1,0:T(8,128)}, u32[]{:S(2)}) copy-start(f32[7,6]{1,0:T(8,128)} %param.39) | copy-start | bytes 508
  94.2 21.7 %all-to-all-start.1 = ((bf16[16,5,1152]{2,1,0:T(8,128)(2,1)}), bf16[16,5,1152]{2,1,0:T(8,128)(2,1)S(1)}, u32[]{:S(2)}, u32[]{:S(2)}) async-start(bf16[16,5,1152]{2,1,0:T(8,128)(2,1)} %all_to_all.19), calls=%async_computation.1 | async-start | bytes 589824 | tf_op jit(solution)/shard_map/all_to_all | solution.py:137
  100.9 13.8 %reduce-scatter.9.cloned.1.call-start = ((), (), s32[]{:S(2)}) async-start(), calls=%async_computation.5 | async-start | bytes 884736
Sparse Core Ops, SparseCore 0:
  86.4 5.7 reduce-scatter.6
  105.4 9.2 reduce-scatter.8
where the time goes:
time: 125 us; the launch traced here: 124 us
  matrix products  34.1 us (27%)
  local copies, waits for them, and re-layouts  26.8 us (21%)
  blocking collectives  24.9 us (20%)
  between operations  13.7 us (11%)
  waiting for transfers between devices  13.1 us (10%)
  starting transfers between devices  6.78 us (5%)
  other arithmetic  4.34 us (3%)
    unnamed x31, local copies, waits for them, and re-layouts  25.1 us
    all_to_all x1, blocking collectives, shards(): lax.all_to_all(send_slice, 'ep', split_axis=0, concat_axis=0, tiled=True)  19 us
    unnamed x4, waiting for transfers between devices  13.1 us
    dot_general x1, matrix products, shards(): jnp.einsum('shj,sjhv->shv', mixture, cache_values, preferred_element_type...  7.61 us
    dot_general x1, matrix products, shards(): jnp.einsum('shmd,sjhmd->shmj', queries, past_keys, preferred_element_type...  7.34 us
    all_to_all x1, starting transfers between devices, shards(): lax.all_to_all(expert_sum.astype(jnp.bfloat16), 'ep', split_axis=0, conca...  6.73 us
    psum x1, blocking collectives, shards(): lax.psum(attn_part.astype(jnp.bfloat16), 'tp').astype(jnp.float32)  3.78 us
    dot_general x1, matrix products, shards(): jnp.dot(shared_hidden, shared_down, preferred_element_type=jnp.float32)  3.2 us
  transfers between devices with their start and end apart: 3, of which 2 were waited for; matrix products, arithmetic and copies ran while one was open for 6% of the time, Pallas kernels for 0%

commit v1 on v0

--- a/solution.py
+++ b/solution.py
@@ -87,7 +87,9 @@
     attn_part = lax.dot_general(
         head_normed, out_weight, (((1,), (1,)), ((), ())), preferred_element_type=jnp.float32
     )
-    attn_total = lax.psum(attn_part.astype(jnp.bfloat16), "tp").astype(jnp.float32)
+    attn_total = jnp.sum(lax.all_gather(attn_part.astype(jnp.bfloat16), "tp"), axis=0).astype(
+        jnp.float32
+    )
     mixed_rows = (tokens.astype(jnp.float32) + attn_total).astype(jnp.bfloat16)
     moe_normed = rms_scale(mixed_rows, moe_gain).astype(jnp.bfloat16)
     shared_gate_out = jnp.dot(moe_normed, shared_gate, preferred_element_type=jnp.float32)

time: 125 us -> 123 us (0.984)
  blocking collectives: 24.9 us -> 23.1 us
    psum x1 -> x0, blocking collectives: 3.78 us -> none  [shards(): lax.psum(attn_part.astype(jnp.bfloat16), 'tp').astype(jnp.float32)]
    all_gather x0 -> x1, blocking collectives: none -> 2.01 us  [shards(): lax.all_gather(attn_part.astype(jnp.bfloat16), 'tp')]
where the time goes in v1:
time: 123 us; the launch traced here: 122 us
  matrix products  34.1 us (28%)
  local copies, waits for them, and re-layouts  26.8 us (22%)
  blocking collectives  23.1 us (19%)
  between operations  13.7 us (11%)
  waiting for transfers between devices  13.1 us (11%)
  starting transfers between devices  6.78 us (6%)
  other arithmetic  4.36 us (4%)
    unnamed x31, local copies, waits for them, and re-layouts  25.1 us
    all_to_all x1, blocking collectives, shards(): lax.all_to_all(send_slice, 'ep', split_axis=0, concat_axis=0, tiled=True)  19 us
    unnamed x4, waiting for transfers between devices  13.1 us
    dot_general x1, matrix products, shards(): jnp.einsum('shj,sjhv->shv', mixture, cache_values, preferred_element_type...  7.61 us
    dot_general x1, matrix products, shards(): jnp.einsum('shmd,sjhmd->shmj', queries, past_keys, preferred_element_type...  7.34 us
    all_to_all x1, starting transfers between devices, shards(): lax.all_to_all(expert_sum.astype(jnp.bfloat16), 'ep', split_axis=0, conca...  6.74 us
    dot_general x1, matrix products, shards(): jnp.dot(shared_hidden, shared_down, preferred_element_type=jnp.float32)  3.2 us
    dot_general x1, matrix products, shards(): jnp.dot(normed, key_weight, preferred_element_type=jnp.float32)  3.15 us
  transfers between devices with their start and end apart: 3, of which 2 were waited for; matrix products, arithmetic and copies ran while one was open for 6% of the time, Pallas kernels for 0%

profile of v1, /device:TPU:0, one launch (start us, length us, event | category | flops | bytes accessed | tf_op | source)
XLA Modules:
  0.0 121.9 jit_solution(9992183582123899538)
XLA Ops:
  6.5 0.0 copy-start
  6.5 0.0 reduce-scatter.7.cloned.1.call-start
  6.5 0.8 convert_element_type.104
  7.4 0.9 fusion.37
  8.3 3.1 %convolution_convert_fusion.6 = bf16[7,1024]{1,0:T(8,128)(2,1)S(1)} fusion(bf16[2304,1024]{1,0:T(8,128)(2,1)} %param.22, bf16[7,2304]{1,0:T(8,128)(2,1)} %param.20, f32[2304]{0:T(1024)S(1)} %convert_element_type.104, f32[7]{0:T(128)S(1)} %add_rsqrt_fusion.2), kind=kOutput, calls=%fused_computation.21 | convolution fusion | flops 33101824 | bytes 4774428 | tf_op jit(solution)/shard_map/dot_general | solution.py:45
  11.4 0.1 reshape.150
  11.5 0.1 reshape.134
  11.6 0.0 copy-start.1
  11.6 20.6 %copy.40 = bf16[7,1024,8,128]{1,3,2,0:T(8,128)(2,1)} copy(bf16[7,1024,8,128]{3,2,1,0:T(8,128)(2,1)} %param.28) | data formatting | bytes 29360128 | tf_op args[8]
  32.2 0.0 copy-done.6
  32.2 0.1 iota_compare_fusion
  32.3 3.1 %fusion.19 = f32[7,1024]{1,0:T(8,128)S(1)} fusion(bf16[2304,1024]{1,0:T(8,128)(2,1)} %param.23, bf16[7,2304]{1,0:T(8,128)(2,1)S(1)} %copy-done.1, f32[2304]{0:T(1024)S(1)} %convert_element_type.104, f32[7]{0:T(128)S(1)} %add_rsqrt_fusion.2), kind=kOutput, calls=%fused_computation.20 | convolution fusion | flops 33108992 | bytes 4788764 | tf_op jit(solution)/shard_map/dot_general | solution.py:48
  35.4 0.1 reshape.137
  35.5 0.1 multiply_reduce_fusion
  35.7 0.1 copy.41
  35.8 7.3 %fusion.70 = f32[7,8,2,1,1024]{4,3,2,1,0:T(1,128)S(1)} fusion(bf16[7,8,2,64,1]{3,4,2,1,0:T(2,128)(2,1)S(1)} %reshape.150, bf16[7,1024,8,2,64]{1,4,3,2,0:T(8,128)(2,1)} %bitcast.89), kind=kOutput, calls=%fused_computation.102 | convolution fusion | flops 14680064 | bytes 15153152 | tf_op jit(solution)/shard_map/shmd,sjhmd->shmj/dot_general | solution.py:58
  43.1 0.3 select_reduce_fusion
  43.4 0.3 fusion.22
  43.7 0.2 fusion.21
  44.0 0.1 fusion.32
  44.2 0.0 slice-start.2
  44.2 0.8 fusion.18
  44.9 7.6 %fusion = f32[7,8,1,128]{3,2,1,0:T(1,128)S(1)} fusion(bf16[7,1024,8,128]{3,2,1,0:T(8,128)(2,1)} %param.29, bf16[7,8,1024,1]{2,1,0,3:T(8,128)(2,1)S(1)} %fusion.32), kind=kOutput, calls=%fused_computation | convolution fusion | flops 14680064 | bytes 14823424 | tf_op jit(solution)/shard_map/shj,sjhv->shv/dot_general | solution.py:76
  52.6 0.0 copy-start.3
  52.6 0.0 copy-start.2
  52.6 0.2 multiply_reduce_fusion.1
  52.7 0.0 copy-done.7
  52.8 0.1 fusion.53
  52.9 1.3 %fusion.2 = bf16[1,7,2304]{2,1,0:T(8,128)(2,1)S(1)} fusion(bf16[2304,1024]{1,0:T(8,128)(2,1)S(1)} %bitcast.93, bf16[1,7,8,128]{3,2,1,0:T(8,128)(2,1)S(1)} %fusion.53), kind=kOutput, calls=%fused_computation.5 | convolution fusion | flops 33046272 | bytes 4765184 | tf_op jit(solution)/shard_map/dot_general | solution.py:87
  54.2 2.0 %all-gather.1 = bf16[2,7,2304]{2,1,0:T(8,128)(2,1)S(1)} all-gather(bf16[1,7,2304]{2,1,0:T(8,128)(2,1)S(1)} %fusion.2), channel_id=2, replica_groups=mesh['ep'=16,'tp'=2] {'tp'}, dimensions={0}, use_global_device_ids=true | all-gather | bytes 96768 | tf_op jit(solution)/shard_map/all_gather | solution.py:90
  56.2 0.1 fusion.34
  56.4 0.1 eq.63
  56.5 0.1 fusion.42
  56.6 0.1 reduce_window_sum.11
  56.6 0.2 select_reduce_fusion.1
  56.8 0.1 fusion.36
  56.9 0.5 convolution_convert_fusion.3
  57.4 0.1 all_to_all.16
  57.5 19.0 %all_to_all.24 = bf16[16,5,1152]{2,1,0:T(8,128)(2,1)S(1)} all-to-all(bf16[16,5,1152]{2,1,0:T(8,128)(2,1)S(1)} %all_to_all.16), channel_id=1, replica_groups=mesh['ep'=16,'tp'=2] {'ep'}, dimensions={0} | all-to-all | bytes 368640 | tf_op jit(solution)/shard_map/all_to_all | solution.py:125
  76.5 0.1 all_to_all.18
  76.6 2.1 %all_gather.11 = bf16[80,2304]{1,0:T(8,128)(2,1)S(1)} all-gather(bf16[80,1152]{1,0:T(8,128)(2,1)S(1)} %all_to_all.18), channel_id=1, replica_groups=mesh['ep'=16,'tp'=2] {'tp'}, dimensions={1}, use_global_device_ids=true | all-gather | bytes 552960 | tf_op jit(solution)/shard_map/all_gather | solution.py:126
  78.7 2.2 %fusion.6 = f32[80,512]{1,0:T(8,128)S(1)} fusion(bf16[80,2304]{1,0:T(8,128)(2,1)S(1)} %all_gather.11, bf16[1,2304,512]{2,1,0:T(8,128)(2,1)} %param.32), kind=kOutput, calls=%fused_computation.9 | convolution fusion | flops 188743680 | bytes 2891776 | tf_op jit(solution)/shard_map/dot_general | solution.py:127
  80.8 2.6 %convolution_convert_fusion = bf16[80,2304]{1,0:T(8,128)(2,1)S(1)} fusion(bf16[1,512,2304]{2,1,0:T(8,128)(2,1)S(1)} %copy-done, bf16[80,2304]{1,0:T(8,128)(2,1)S(1)} %all_gather.11, bf16[1,2304,512]{2,1,0:T(8,128)(2,1)} %param.33, f32[80,512]{1,0:T(8,128)S(1)} %fusion.6), kind=kOutput, calls=%fused_computation.2 | convolution fusion | flops 377917440 | bytes 5619712 | tf_op jit(solution)/shard_map/dot_general | solution.py:130
  83.5 1.1 copy.50
  84.5 0.0 reduce-scatter.7.cloned.1.call-update
  84.6 0.0 copy-start.4
  84.6 2.1 %fusion.71 = f32[7,512]{1,0:T(8,128)S(1)} fusion(bf16[7,2304]{1,0:T(8,128)(2,1)S(1)} %fusion.36, bf16[2304,512]{1,0:T(8,128)(2,1)} %param.35), kind=kOutput, calls=%fused_computation.103 | convolution fusion | flops 16515072 | bytes 2405888 | tf_op jit(solution)/shard_map/dot_general | solution.py:95
  86.6 3.9 %reduce-scatter.7.cloned.1.call-done = bf16[1152,80]{1,0:T(8,128)(2,1)} async-done(((bf16[2304,80]{1,0:T(8,128)(2,1)}), bf16[1152,80]{1,0:T(8,128)(2,1)}) %reduce-scatter.7.cloned.1.call-update) | async-done | bytes 184336
  90.5 1.1 copy.51
  91.6 0.8 all_to_all.19
  92.4 6.7 %all-to-all-start.1 = ((bf16[16,5,1152]{2,1,0:T(8,128)(2,1)}), bf16[16,5,1152]{2,1,0:T(8,128)(2,1)S(1)}, u32[]{:S(2)}, u32[]{:S(2)}) async-start(bf16[16,5,1152]{2,1,0:T(8,128)(2,1)} %all_to_all.19), calls=%async_computation.1 | async-start | bytes 589824 | tf_op jit(solution)/shard_map/all_to_all | solution.py:139
  99.2 0.0 reduce-scatter.9.cloned.1.call-start
  99.2 3.2 %convolution_convert_fusion.1 = bf16[7,2304]{1,0:T(8,128)(2,1)S(1)} fusion(bf16[512,2304]{1,0:T(8,128)(2,1)} %param.37, bf16[7,2304]{1,0:T(8,128)(2,1)S(1)} %fusion.36, bf16[2304,512]{1,0:T(8,128)(2,1)} %param.36, f32[7,512]{1,0:T(8,128)S(1)} %fusion.71), kind=kOutput, calls=%fused_computation.3 | convolution fusion | flops 33067776 | bytes 4797440 | tf_op jit(solution)/shard_map/dot_general | solution.py:98
  102.4 1.1 copy.52
  103.5 0.0 reduce-scatter.9.cloned.1.call-update
  103.6 0.1 reduce_sum.83
  103.6 0.1 copy.44
  103.7 0.1 copy.43
  103.8 9.2 %reduce-scatter.9.cloned.1.call-done = bf16[1152,7]{1,0:T(8,128)(2,1)} async-done(((bf16[2304,7]{1,0:T(8,128)(2,1)}), bf16[1152,7]{1,0:T(8,128)(2,1)}) %reduce-scatter.9.cloned.1.call-update) | async-done | bytes 16144
  113.0 1.1 copy.53
  114.1 0.0 all-to-all-done.1
  114.1 0.1 reshape.148
  114.2 0.2 fusion.11
  114.5 0.6 add_convert_fusion
  (30 shorter events, 0.1 us)
Async XLA Ops:
  6.5 74.3 %copy-start = (bf16[1,512,2304]{2,1,0:T(8,128)(2,1)S(1)}, bf16[1,512,2304]{2,1,0:T(8,128)(2,1)}, u32[]{:S(2)}) copy-start(bf16[1,512,2304]{2,1,0:T(8,128)(2,1)} %param.34) | copy-start | bytes 7077892
  6.5 84.0 %reduce-scatter.7.cloned.1.call-start = ((), (), s32[]{:S(2)}) async-start(), calls=%async_computation.4 | async-start | bytes 884736
  11.6 20.6 %copy-start.6 = (s32[7]{0:T(128)S(1)}, s32[7]{0:T(128)}, u32[]{:S(2)}) copy-start(s32[7]{0:T(128)} %param.30) | copy-start | bytes 88
  11.6 20.7 %copy-start.1 = (bf16[7,2304]{1,0:T(8,128)(2,1)S(1)}, bf16[7,2304]{1,0:T(8,128)(2,1)}, u32[]{:S(2)}) copy-start(bf16[7,2304]{1,0:T(8,128)(2,1)} %param.20) | copy-start | bytes 96772
  32.3 11.9 %slice-start = ((s8[4718592]{0:T(1024)(128)(4,1)}), s8[524288]{0:T(1024)(128)(4,1)S(1)}, s32[]{:S(2)}) async-start(s8[4718592]{0:T(1024)(128)(4,1)} %bitcast.90), calls=%async_computation.6 | async-start | bytes 1048576
  35.8 8.2 %copy-start.5 = (f32[8]{0:T(128)S(1)}, f32[8]{0:T(128)}, u32[]{:S(2)}) copy-start(f32[8]{0:T(128)} %param.26) | copy-start | bytes 100
  35.8 8.3 %slice-start.1 = ((s8[4718592]{0:T(1024)(128)(4,1)}), s8[4194304]{0:T(1024)(128)(4,1)S(1)}, s32[]{:S(2)}) async-start(s8[4718592]{0:T(1024)(128)(4,1)} %bitcast.90), calls=%async_computation.7 | async-start | bytes 8388608
  44.2 8.7 %slice-start.2 = ((s8[4718592]{0:T(1024)(128)(4,1)}), s8[4194304]{0:T(1024)(128)(4,1)S(1)}, s32[]{:S(2)}) async-start(s8[4718592]{0:T(1024)(128)(4,1)} %bitcast.92), calls=%async_computation.8 | async-start | bytes 8388608
  44.9 7.8 %copy-start.7 = (bf16[128]{0:T(256)(128)(2,1)S(1)}, bf16[128]{0:T(256)(128)(2,1)}, u32[]{:S(2)}) copy-start(bf16[128]{0:T(256)(128)(2,1)} %param.27) | copy-start | bytes 772
  44.9 7.9 %slice-start.3 = ((s8[4718592]{0:T(1024)(128)(4,1)}), s8[524288]{0:T(1024)(128)(4,1)S(1)}, s32[]{:S(2)}) async-start(s8[4718592]{0:T(1024)(128)(4,1)} %bitcast.92), calls=%async_computation.9 | async-start | bytes 1048576
  52.6 3.8 %copy-start.3 = (bf16[2304]{0:T(1024)(128)(2,1)S(1)}, bf16[2304]{0:T(1024)(128)(2,1)}, u32[]{:S(2)}) copy-start(bf16[2304]{0:T(1024)(128)(2,1)} %param.31) | copy-start | bytes 13828
  52.6 3.8 %copy-start.2 = (s32[7,6]{1,0:T(8,128)S(1)}, s32[7,6]{1,0:T(8,128)}, u32[]{:S(2)}) copy-start(s32[7,6]{1,0:T(8,128)} %param.38) | copy-start | bytes 508
  84.6 19.2 %copy-start.4 = (f32[7,6]{1,0:T(8,128)S(1)}, f32[7,6]{1,0:T(8,128)}, u32[]{:S(2)}) copy-start(f32[7,6]{1,0:T(8,128)} %param.39) | copy-start | bytes 508
  92.4 21.7 %all-to-all-start.1 = ((bf16[16,5,1152]{2,1,0:T(8,128)(2,1)}), bf16[16,5,1152]{2,1,0:T(8,128)(2,1)S(1)}, u32[]{:S(2)}, u32[]{:S(2)}) async-start(bf16[16,5,1152]{2,1,0:T(8,128)(2,1)} %all_to_all.19), calls=%async_computation.1 | async-start | bytes 589824 | tf_op jit(solution)/shard_map/all_to_all | solution.py:139
  99.2 13.8 %reduce-scatter.9.cloned.1.call-start = ((), (), s32[]{:S(2)}) async-start(), calls=%async_computation.5 | async-start | bytes 884736
Sparse Core Ops, SparseCore 0:
  84.7 5.7 reduce-scatter.6
  103.7 9.2 reduce-scatter.8
